TPU v7x, 32 devices: a whole 2x2x4 slice. The times are simulated.
32 devices in a mesh: gr: 2 (over x), sp: 8 (over z, y), tp: 2 (over core).
Axes of the slice: x: 2, y: 2, z: 4, core: 2. Of those that a mesh axis runs over, the one named last changes fastest.
Arguments:
- tokens: bfloat16 [8, 1024, 4096], P('gr', 'sp'), parts along dimension 0, may hold values from -6 to 6
- key_weight: bfloat16 [4096, 2048], P('sp', 'tp'), may hold values from -0.09375 to 0.09375
- value_weight: bfloat16 [4096, 2048], P('sp', 'tp'), may hold values from -0.09375 to 0.09375
- log_decay: float32 [32, 8, 1024], P('tp', 'gr', 'sp'), parts along dimension 1, may hold values from -1 to 0, as said below
- new_query: bfloat16 [8, 2048], P('gr', 'tp'), parts along dimension 0, may hold values from -6 to 6
- new_key: bfloat16 [8, 2048], P('gr', 'tp'), parts along dimension 0, may hold values from -24 to 24
- new_value: bfloat16 [8, 2048], P('gr', 'tp'), parts along dimension 0, may hold values from -6 to 6
- step_decay: float32 [32, 8], P('tp', 'gr'), parts along dimension 1, may hold values from -1.5 to -0.05
- norm_gain: float32 [2048], P('tp'), may hold values from 0.1 to 1.9
Outputs:
- state_cache: float32 [512, 32, 64], P('gr', 'tp'), parts along dimension 0
- first_read: bfloat16 [8, 2048], P('gr', 'tp'), parts along dimension 0
There are 2 independent parts, one for each index of `gr`. A program takes and returns all parts, laid end to end along the dimension named above; an argument that names none is the same for every part. Nothing has to cross between parts.
Inputs may be any that keep to these rules, and one draw needn't show every extreme that they name: `log_decay`: every entry is at most zero.
All inputs are finite; a program needn't handle non-finite values.
Results may differ from a plain program's by a relative error of at most 0.0053.
Values may be sent and summed in bfloat16 or wider, within the bound.
A program may use at most 64 MiB of HBM per device.

v0:
```python
import jax
import jax.numpy as jnp
from jax import lax
from jax.sharding import PartitionSpec as P

HEAD_DIM = 64


def entering(x, axis, combine, identity):
    devices, mine = (lax.axis_size(axis), lax.axis_index(axis))
    everything = lax.all_gather(x, axis)
    start = jnp.broadcast_to(jnp.asarray(identity, x.dtype), x.shape)

    def lap(k, before):
        at = devices - 1 - k
        reached = at > mine
        new = combine(before, everything[at])
        return jnp.where(reached, new, before)

    return lax.fori_loop(0, devices, lap, start)


def rotate_half(values, positions):
    half = values.shape[-1] // 2
    inverse = 10000.0 ** (-jnp.arange(half, dtype=jnp.float32) * (2.0 / values.shape[-1]))
    angles = positions[..., None] * inverse
    cosine = jnp.cos(angles)
    sine = jnp.sin(angles)
    first, second = (values[..., :half], values[..., half:])
    return jnp.concatenate(
        [first * cosine - second * sine, second * cosine + first * sine], axis=-1
    )


def add_totals(earlier, later):
    return earlier + later


def shards(
    tokens,
    key_weight,
    value_weight,
    log_decay,
    new_query,
    new_key,
    new_value,
    step_decay,
    norm_gain,
):
    seqs, span, width = tokens.shape
    heads_here = key_weight.shape[1] // HEAD_DIM
    token_rows = tokens.reshape(seqs * span, width)
    whole_keys, whole_values = (
        lax.all_gather(key_weight, "sp", axis=0, tiled=True),
        lax.all_gather(value_weight, "sp", axis=0, tiled=True),
    )
    key_sum = jnp.dot(token_rows, whole_keys, preferred_element_type=jnp.float32)
    value_sum = jnp.dot(token_rows, whole_values, preferred_element_type=jnp.float32)
    key_vectors = (
        lax.optimization_barrier(key_sum.astype(jnp.bfloat16))
        .astype(jnp.float32)
        .reshape(seqs, span, heads_here, HEAD_DIM)
    )
    values = (
        lax.optimization_barrier(value_sum.astype(jnp.bfloat16))
        .astype(jnp.float32)
        .reshape(seqs, span, heads_here, HEAD_DIM)
    )
    devices = lax.axis_size("sp")
    offset = lax.axis_index("sp") * span
    positions = (offset + jnp.arange(span, dtype=jnp.int32)).astype(jnp.float32)
    rkeys = rotate_half(key_vectors, positions[None, :, None]) * HEAD_DIM ** (-0.5)
    totals = jnp.sum(log_decay, axis=-1)
    later_sum = entering(totals, "sp", add_totals, jnp.zeros_like(totals))
    weight = jnp.exp(totals[:, :, None] - jnp.cumsum(log_decay, axis=-1) + later_sum[:, :, None])
    weighted = rkeys * jnp.transpose(weight, (1, 2, 0))[:, :, :, None]
    term = jnp.einsum("stha,sthb->sahb", weighted, values, precision=lax.Precision.HIGHEST)
    term = term.reshape(seqs * HEAD_DIM, heads_here, HEAD_DIM)
    end_pos = jnp.full((seqs, heads_here), float(span * devices), jnp.float32)
    query = rotate_half(new_query.astype(jnp.float32).reshape(seqs, heads_here, HEAD_DIM), end_pos)
    key_new = rotate_half(
        new_key.astype(jnp.float32).reshape(seqs, heads_here, HEAD_DIM), end_pos
    ) * HEAD_DIM ** (-0.5)
    value_new = new_value.astype(jnp.float32).reshape(seqs, heads_here, HEAD_DIM)
    decay_all = jnp.repeat(jnp.exp(step_decay).T, HEAD_DIM, axis=0)
    key_all = jnp.transpose(key_new, (0, 2, 1)).reshape(seqs * HEAD_DIM, heads_here)
    value_all = jnp.repeat(value_new, HEAD_DIM, axis=0)
    summed = lax.psum(term, "sp")
    state_cache = decay_all[:, :, None] * summed + key_all[:, :, None] * value_all
    state_seq = state_cache.reshape(seqs, HEAD_DIM, heads_here, HEAD_DIM)
    raw = jnp.einsum("sha,sahb->shb", query, state_seq, precision=lax.Precision.HIGHEST)
    center = jnp.mean(raw, axis=-1, keepdims=True)
    spread = jnp.mean(jnp.square(raw - center), axis=-1, keepdims=True)
    normed = (raw - center) * lax.rsqrt(spread + 1e-06) * norm_gain.reshape(heads_here, HEAD_DIM)
    first_read = normed.reshape(seqs, heads_here * HEAD_DIM).astype(jnp.bfloat16)
    return (state_cache, first_read)


def solution(mesh):
    placed = (
        P("gr", "sp", None),
        P("sp", "tp"),
        P("sp", "tp"),
        P("tp", "gr", "sp"),
        P("gr", "tp"),
        P("gr", "tp"),
        P("gr", "tp"),
        P("tp", "gr"),
        P("tp"),
    )
    return jax.shard_map(
        shards,
        mesh=mesh,
        in_specs=placed,
        out_specs=(P("gr", "tp", None), P("gr", "tp")),
        check_vma=False,
    )
```

profile of v0, /device:TPU:0, one launch (start us, length us, event | category | flops | bytes accessed | tf_op | source)
XLA Modules:
  0.0 378.3 jit_solution(3645071348651051041)
XLA Ops:
  7.2 0.7 all-gather.7.cloned.1.call-update
  8.0 0.7 all-gather.5.cloned.1.call-update
  9.0 1.1 reduce_window_sum.13
  10.1 28.8 %all-gather.1 = f32[8,16,4]{1,2,0:T(4,128)S(1)} all-gather(f32[1,16,4]{1,2,0:T(4,128)S(1)} %bitcast.52), channel_id=2, replica_groups=mesh['gr'=2,'sp'=8,'tp'=2] {'sp'}, dimensions={0}, use_global_device_ids=true | all-gather | bytes 2304 | tf_op jit(solution)/shard_map/all_gather | solution.py:11
  38.9 0.3 while.16
  39.2 0.1 fusion.13
  39.4 0.1 multiply_cosine_fusion
  39.5 98.0 %all-gather.7.cloned.1.call-done = bf16[4096,1024]{1,0:T(8,128)(2,1)} async-done(((bf16[512,1024]{1,0:T(8,128)(2,1)}), bf16[4096,1024]{1,0:T(8,128)(2,1)}) %all-gather.7.cloned.1.call-update) | async-done | bytes 8388624 | tf_op jit(solution)/shard_map/all_gather | solution.py:54
  137.5 9.1 %convolution_convert_fusion = bf16[512,1024]{1,0:T(8,128)(2,1)S(1)} fusion(bf16[512,4096]{1,0:T(8,128)(2,1)} %bitcast.53, bf16[4096,1024]{1,0:T(8,128)(2,1)} %all-gather.7.cloned.1.call-done), kind=kOutput, calls=%fused_computation.8 | convolution fusion | flops 4295491584 | bytes 13631488 | tf_op jit(solution)/shard_map/dot_general | solution.py:57
  146.6 115.7 %all-gather.5.cloned.1.call-done = bf16[4096,1024]{1,0:T(8,128)(2,1)} async-done(((bf16[512,1024]{1,0:T(8,128)(2,1)}), bf16[4096,1024]{1,0:T(8,128)(2,1)}) %all-gather.5.cloned.1.call-update) | async-done | bytes 8388624 | tf_op jit(solution)/shard_map/all_gather | solution.py:55
  262.3 10.1 %convolution_convert_fusion.1 = bf16[512,1024]{1,0:T(8,128)(2,1)} fusion(bf16[512,4096]{1,0:T(8,128)(2,1)} %bitcast.54, bf16[4096,1024]{1,0:T(8,128)(2,1)} %all-gather.5.cloned.1.call-done), kind=kOutput, calls=%fused_computation.9 | convolution fusion | flops 4295491584 | bytes 13631488 | tf_op jit(solution)/shard_map/dot_general | solution.py:58
  272.4 2.9 reshape.171
  275.4 1.7 copy.30
  277.0 2.9 reshape.158
  279.9 2.1 multiply_subtract_fusion
  282.1 0.6 maximum_multiply_fusion
  282.7 2.1 fusion.5
  284.7 1.4 copy.37
  286.2 2.1 reshape.148
  288.6 0.1 mul.185
  288.9 0.1 multiply_subtract_fusion.1
  289.2 0.2 copy.45
  289.4 1.2 broadcast_in_dim.8
  290.6 1.1 reshape.153
  291.9 73.2 %all-reduce.2.cloned.1.call-done = f32[256,16,64]{0,2,1:T(8,128)} async-done(((f32[256,16,64]{0,2,1:T(8,128)}), f32[256,16,64]{0,2,1:T(8,128)}) %all-reduce.2.cloned.1.call-update) | async-done | bytes 1048592 | tf_op jit(solution)/shard_map/psum | solution.py:88
  365.0 1.4 multiply_add_fusion
  366.4 0.9 reshape.156
  367.3 3.4 fusion.2
  370.7 0.1 reduce_sum.28
  370.8 0.2 multiply_reduce_fusion
  371.0 0.1 multiply_convert_fusion
  371.1 0.7 convert_element_type.28
  (47 shorter events, 1.3 us)
Async XLA Ops:
  7.2 1.6 copy-start.1
  7.2 130.3 %all-gather.7.cloned.1.call-start = ((), (), s32[]{:S(2)}) async-start(), calls=%async_computation.1 | async-start | bytes 9437184 | tf_op jit(solution)/shard_map/all_gather | solution.py:54
  7.9 254.4 %all-gather.5.cloned.1.call-start = ((), (), s32[]{:S(2)}) async-start(), calls=%async_computation | async-start | bytes 9437184 | tf_op jit(solution)/shard_map/all_gather | solution.py:55
  8.7 356.3 %all-reduce.2.cloned.1.call-start = ((), (), s32[]{:S(2)}) async-start(), calls=%async_computation.2 | async-start | bytes 2097152 | tf_op jit(solution)/shard_map/psum | solution.py:88
  286.2 2.2 copy-start.6
  286.2 2.3 copy-start.5
  286.2 2.5 copy-start.3
  286.2 2.6 copy-start.4
  286.2 3.0 copy-start.2
  366.4 4.3 %copy-start = (f32[256,16,64]{0,2,1:T(8,128)}, f32[256,16,64]{0,2,1:T(8,128)S(1)}, u32[]{:S(2)}) copy-start(f32[256,16,64]{0,2,1:T(8,128)S(1)} %multiply_add_fusion) | copy-start | bytes 3145732
Sparse Core Ops, SparseCore 0:
  10.1 127.3 all-gather.6
  139.6 122.6 all-gather.4
  288.5 76.4 all-reduce.1
where the time goes:
time: 379 us; the launch traced here: 378 us
  waiting for transfers between devices  288 us (76%)
  blocking collectives  28.8 us (8%)
  matrix products  24.7 us (7%)
  local copies, waits for them, and re-layouts  16 us (4%)
  between operations  14 us (4%)
  other arithmetic  6.37 us (2%)
    all_gather x1, waiting for transfers between devices, shards(): lax.all_gather(value_weight, 'sp', axis=0, tiled=True)  116 us
    all_gather x1, waiting for transfers between devices, shards(): lax.all_gather(key_weight, 'sp', axis=0, tiled=True)  98 us
    psum x1, waiting for transfers between devices, shards(): summed = lax.psum(term, 'sp')  73.2 us
    all_gather x1, blocking collectives, entering(): everything = lax.all_gather(x, axis)  28.8 us
    dot_general x1, matrix products, shards(): jnp.dot(token_rows, whole_values, preferred_element_type=jnp.float32)  10.1 us
    dot_general x1, matrix products, shards(): jnp.dot(token_rows, whole_keys, preferred_element_type=jnp.float32)  9.14 us
  transfers between devices with their start and end apart: 3, of which 3 were waited for; matrix products, arithmetic and copies ran while one was open for 4% of the time, Pallas kernels for 0%

commit v1 on v0

v1 whole, which is shorter than its diff:
```python
import functools

import jax
import jax.numpy as jnp
from jax import lax
from jax.experimental import pallas as pl
from jax.experimental.pallas import tpu as pltpu
from jax.sharding import PartitionSpec as P

HEAD_DIM = 64
SUB = 2
MESH = pl.DeviceIdType.MESH
F32 = jnp.float32
HIGH = lax.Precision.HIGHEST


def kernel(
    sizes,
    tok, kw, vw, ld, tot, cos_ref, sin_ref,
    out,
    toks, w, keys, vals, lds, tots, part, got, full,
    l_sem, tok_s, tok_r, core_s, core_r, yw_s, yw_r, up_s, dn_s, z_r, x_s, x_r,
    ld_s, ld_r, tot_s, tot_r, rs_s, rs_r, ag_s, ag_r, yg_s, yg_r,
):
    n_sp, seqs, span, heads = sizes
    n_a = n_sp // 2
    g, sp, tp = lax.axis_index("gr"), lax.axis_index("sp"), lax.axis_index("tp")
    a, b = sp // 2, sp % 2
    ob = 1 - b
    core = tp % 2
    mate = tp + 1 - 2 * core
    rows, width = tok.shape
    depth = kw.shape[0]
    cols = kw.shape[1] // 2
    piece = depth // SUB
    half = rows // 2
    hs = heads * seqs
    y_peer = (g, a * 2 + ob, tp)
    x_peer = (1 - g, sp, tp)
    core_peer = (g, sp, mate)

    def mine(col_half):
        return pl.ds(pl.multiple_of(col_half * cols, 128), cols)

    def shard_rows(s, q=None):
        if q is None:
            return pl.ds(pl.multiple_of(s * depth, depth), depth)
        return pl.ds(pl.multiple_of(s * depth + q * piece, piece), piece)

    local = [
        pltpu.make_async_copy(kw.at[:, mine(b)], w.at[0, shard_rows(sp)], l_sem.at[0]),
        pltpu.make_async_copy(vw.at[:, mine(b)], w.at[1, shard_rows(sp)], l_sem.at[1]),
        pltpu.make_async_copy(tok, toks.at[b], l_sem.at[2]),
        pltpu.make_async_copy(ld, lds.at[b], l_sem.at[3]),
        pltpu.make_async_copy(tot, tots.at[sp], l_sem.at[4]),
    ]
    for c in local:
        c.start()

    barrier = pltpu.get_barrier_semaphore()

    @pl.loop(1, n_sp)
    def _(k):
        pl.semaphore_signal(barrier, inc=1, device_id=(g, lax.rem(sp + k, n_sp), tp), device_id_type=MESH)

    pl.semaphore_signal(barrier, inc=1, device_id=x_peer, device_id_type=MESH)
    pl.semaphore_signal(barrier, inc=1, device_id=core_peer, device_id_type=MESH)
    pl.semaphore_wait(barrier, n_sp + 1)

    def remote(src, dst, s, r, dev):
        return pltpu.make_async_remote_copy(
            src_ref=src, dst_ref=dst, send_sem=s, recv_sem=r, device_id=dev, device_id_type=MESH
        )

    def yw(m, q):
        src = (kw, vw)[m].at[pl.ds(q * piece, piece), mine(ob)]
        return remote(src, w.at[m, shard_rows(sp, q)], yw_s.at[m, q], yw_r.at[m, q], y_peer)

    half_rows = pl.ds(pl.multiple_of(core * half, half), half)
    ytok = remote(tok.at[half_rows], toks.at[b, half_rows], tok_s, tok_r, y_peer)
    yld = remote(ld, lds.at[b], ld_s, ld_r, y_peer)

    for m in range(2):
        @pl.when(g == m)
        def _():
            for q in range(SUB):
                yw(m, q).start()
            yld.start()
            ytok.start()
            for q in range(SUB):
                yw(1 - m, q).start()

    local[0].wait()
    local[1].wait()

    def zsend(s, q, up):
        ref = w.at[g, shard_rows(s, q)]
        sem = (up_s if up else dn_s).at[s, q]
        return remote(ref, ref, sem, z_r.at[s, q], (g, sp + (2 if up else -2), tp))

    def xsend(s, q):
        ref = w.at[g, shard_rows(s, q)]
        return remote(ref, ref, x_s.at[s, q], x_r.at[s, q], x_peer)

    def xrecv(s, q):
        ref = w.at[1 - g, shard_rows(s, q)]
        return remote(ref, ref, x_s.at[s, q], x_r.at[s, q], x_peer)

    def launch(s, q):
        @pl.when(a < n_a - 1)
        def _():
            zsend(s, q, True).start()

        @pl.when(a > 0)
        def _():
            zsend(s, q, False).start()

    for q in range(SUB):
        launch(sp, q)
    local[4].wait()

    def tsend(k):
        return remote(tots.at[sp], tots.at[sp], tot_s.at[k], tot_r.at[k], (g, lax.rem(sp + k, n_sp), tp))

    @pl.loop(1, n_sp)
    def _(k):
        tsend(k).start()

    for q in range(SUB):
        for m in range(2):
            @pl.when(g == m)
            def _():
                yw(m, q).wait_recv()
        launch(a * 2 + ob, q)

    @pl.loop(1, n_a)
    def _(d):
        for bb in range(2):
            for q in range(SUB):
                below = (a - d) * 2 + (b if bb == 0 else ob)
                above = (a + d) * 2 + (b if bb == 0 else ob)

                @pl.when(a - d >= 0)
                def _():
                    zsend(below, q, True).wait_recv()

                    @pl.when(a < n_a - 1)
                    def _():
                        zsend(below, q, True).start()

                    xsend(below, q).start()

                @pl.when(a + d < n_a)
                def _():
                    zsend(above, q, False).wait_recv()

                    @pl.when(a > 0)
                    def _():
                        zsend(above, q, False).start()

                    xsend(above, q).start()

    ytok_in = remote(toks.at[ob, half_rows], toks.at[ob, half_rows], tok_s, tok_r, y_peer)
    ctok = remote(toks.at[ob, half_rows], toks.at[ob, half_rows], core_s, core_r, core_peer)
    ytok_in.wait_recv()
    ctok.start()
    yld.wait_recv()

    @pl.loop(1, n_sp)
    def _(k):
        tsend(k).wait_recv()

    for c in local[2:4]:
        c.wait()

    pos_t = lax.broadcasted_iota(jnp.int32, (span, span), 0)
    pos_u = lax.broadcasted_iota(jnp.int32, (span, span), 1)
    later_mask = jnp.where(pos_u > pos_t, 1.0, 0.0).astype(F32)
    suffix = []
    for tb in range(2):
        inside = lax.dot_general(
            later_mask, lds[tb], (((1,), (1,)), ((), ())), precision=HIGH, preferred_element_type=F32
        )
        index = a * 2 + tb

        def add(k, total):
            return total + jnp.where(k > index, tots[k], 0.0)

        after = lax.fori_loop(0, n_sp, add, jnp.zeros(tots.shape[1:], F32))
        suffix.append(inside + after[0:1, :hs])
    row_hs = lax.broadcasted_iota(jnp.int32, (hs, cols), 0)
    lane_head = lax.broadcasted_iota(jnp.int32, (hs, cols), 1) // HEAD_DIM + b * (heads // 2)

    ctok.wait_recv()

    @pl.loop(1, n_a)
    def _(d):
        for bb in range(2):
            for q in range(SUB):
                @pl.when(a - d >= 0)
                def _():
                    xrecv((a - d) * 2 + (b if bb == 0 else ob), q).wait_recv()

                @pl.when(a + d < n_a)
                def _():
                    xrecv((a + d) * 2 + (b if bb == 0 else ob), q).wait_recv()

    for q in range(SUB):
        for m in range(2):
            @pl.when(g == m)
            def _():
                yw(1 - m, q).wait_recv()

    tile = min(256, rows)
    for tb in range(2):
        @pl.loop(0, rows // tile)
        def _(r):
            at = pl.ds(pl.multiple_of(r * tile, tile), tile)
            lhs = toks[tb, at, :]
            keys[tb, at, :] = jnp.dot(lhs, w[0], preferred_element_type=F32).astype(jnp.bfloat16)
            vals[tb, at, :] = jnp.dot(lhs, w[1], preferred_element_type=F32).astype(jnp.bfloat16)

    lane = lax.broadcasted_iota(jnp.int32, (span, 128), 1)
    first = lane % HEAD_DIM < HEAD_DIM // 2
    lane_out = lax.broadcasted_iota(jnp.int32, (HEAD_DIM, 128), 1)
    block = seqs * HEAD_DIM // n_a
    for s in range(seqs):
        select = jnp.where(row_hs == lane_head * seqs + s, 1.0, 0.0).astype(F32)
        weights = [
            jnp.exp(jnp.dot(suffix[tb], select, precision=HIGH, preferred_element_type=F32))
            for tb in range(2)
        ]
        for c0 in range(0, cols, 128):
            total = None
            for tb in range(2):
                at = pl.ds(s * span, span)
                u = keys[tb, at, pl.ds(c0, 128)].astype(F32)
                turned = jnp.where(first, pltpu.roll(u, 128 - 32, 1), pltpu.roll(u, 32, 1))
                spot = pl.ds(tb * span, span)
                rk = u * cos_ref[spot, :] + turned * sin_ref[spot, :]
                weighted = (rk * weights[tb][:, c0:c0 + 128]).astype(jnp.bfloat16)
                term = lax.dot_general(
                    weighted, vals[tb, at, pl.ds(c0, 128)], (((0,), (0,)), ((), ())),
                    preferred_element_type=F32,
                )
                total = term if total is None else total + term
            both = jnp.where(lane_out < HEAD_DIM, total[:HEAD_DIM], total[HEAD_DIM:])
            part[pl.ds(s * HEAD_DIM, HEAD_DIM), pl.ds(c0, 128)] = both.astype(jnp.bfloat16)

    def block_of(k):
        return pl.ds(pl.multiple_of(k * block, block), block)

    def rs(k):
        to = lax.rem(a + k, n_a)
        return remote(part.at[block_of(to)], got.at[k], rs_s.at[k], rs_r.at[k], (g, to * 2 + b, tp))

    @pl.loop(1, n_a)
    def _(k):
        rs(k).start()

    @pl.loop(1, n_a)
    def _(k):
        rs(k).wait_recv()

    def gather(k, total):
        return total + got[k].astype(F32)

    reduced = lax.fori_loop(1, n_a, gather, part[block_of(a), :].astype(F32))
    full[b, block_of(a), :] = reduced.astype(jnp.bfloat16)

    def ag(k):
        here = full.at[b, block_of(a)]
        return remote(here, here, ag_s.at[k], ag_r.at[k], (g, lax.rem(a + k, n_a) * 2 + b, tp))

    def ag_in(k):
        here = full.at[b, block_of(lax.rem(a - k + n_a, n_a))]
        return remote(here, here, ag_s.at[k], ag_r.at[k], y_peer)

    def yg(k, bb):
        here = full.at[bb, block_of(lax.rem(a - k + n_a, n_a))]
        return remote(here, here, yg_s.at[k], yg_r.at[k], y_peer)

    @pl.loop(1, n_a)
    def _(k):
        ag(k).start()

    yg(0, b).start()

    @pl.loop(1, n_a)
    def _(k):
        ag_in(k).wait_recv()
        yg(k, b).start()

    @pl.loop(0, n_a)
    def _(k):
        yg(k, ob).wait_recv()

    out[:, 0:cols] = full[0]
    out[:, cols:2 * cols] = full[1]

    @pl.loop(0, n_a)
    def _(k):
        yg(k, b).wait_send()

    @pl.loop(1, n_a)
    def _(k):
        ag(k).wait_send()
        rs(k).wait_send()

    @pl.loop(1, n_sp)
    def _(k):
        tsend(k).wait_send()

    ytok.wait_send()
    yld.wait_send()
    ctok.wait_send()
    for q in range(SUB):
        for m in range(2):
            yw(m, q).wait_send()
        for s in (sp, a * 2 + ob):
            @pl.when(a < n_a - 1)
            def _():
                zsend(s, q, True).wait_send()

            @pl.when(a > 0)
            def _():
                zsend(s, q, False).wait_send()

    @pl.loop(1, n_a)
    def _(d):
        for bb in range(2):
            for q in range(SUB):
                below = (a - d) * 2 + (b if bb == 0 else ob)
                above = (a + d) * 2 + (b if bb == 0 else ob)

                @pl.when(a - d >= 0)
                def _():
                    @pl.when(a < n_a - 1)
                    def _():
                        zsend(below, q, True).wait_send()

                    xsend(below, q).wait_send()

                @pl.when(a + d < n_a)
                def _():
                    @pl.when(a > 0)
                    def _():
                        zsend(above, q, False).wait_send()

                    xsend(above, q).wait_send()


def prompt_states(token_rows, key_weight, value_weight, decays, totals, cos, sin, seqs, span, heads, n_sp):
    rows, width = token_rows.shape
    depth, whole = key_weight.shape
    cols = whole // 2
    n_a = n_sp // 2
    hs = heads * seqs
    state_rows = seqs * HEAD_DIM
    dma = pltpu.SemaphoreType.DMA
    bf16 = jnp.bfloat16
    hbm = pl.BlockSpec(memory_space=pl.ANY)
    vmem = pl.BlockSpec(memory_space=pltpu.VMEM)
    return pl.pallas_call(
        functools.partial(kernel, (n_sp, seqs, span, heads)),
        out_shape=jax.ShapeDtypeStruct((state_rows, whole), bf16),
        in_specs=[hbm, hbm, hbm, hbm, hbm, vmem, vmem],
        out_specs=vmem,
        scratch_shapes=[
            pltpu.VMEM((2, rows, width), bf16),
            pltpu.VMEM((2, n_sp * depth, cols), bf16),
            pltpu.VMEM((2, rows, cols), bf16),
            pltpu.VMEM((2, rows, cols), bf16),
            pltpu.VMEM((2, hs, span), F32),
            pltpu.VMEM((n_sp, 8, 128), F32),
            pltpu.VMEM((state_rows, cols), bf16),
            pltpu.VMEM((n_a, state_rows // n_a, cols), bf16),
            pltpu.VMEM((2, state_rows, cols), bf16),
            dma((5,)), dma, dma, dma, dma,
            dma((2, SUB)), dma((2, SUB)),
            dma((n_sp, SUB)), dma((n_sp, SUB)), dma((n_sp, SUB)),
            dma((n_sp, SUB)), dma((n_sp, SUB)),
            dma, dma, dma((n_sp,)), dma((n_sp,)),
            dma((n_a,)), dma((n_a,)), dma((n_a,)), dma((n_a,)), dma((n_a,)), dma((n_a,)),
        ],
        compiler_params=pltpu.CompilerParams(
            collective_id=0, has_side_effects=True, vmem_limit_bytes=56 * 1024 * 1024
        ),
    )(token_rows, key_weight, value_weight, decays, totals, cos, sin)


def rotate_half(values, positions):
    half = values.shape[-1] // 2
    inverse = 10000.0 ** (-jnp.arange(half, dtype=jnp.float32) * (2.0 / values.shape[-1]))
    angles = positions[..., None] * inverse
    cosine = jnp.cos(angles)
    sine = jnp.sin(angles)
    first, second = (values[..., :half], values[..., half:])
    return jnp.concatenate(
        [first * cosine - second * sine, second * cosine + first * sine], axis=-1
    )


def shards(
    tokens, key_weight, value_weight, log_decay, new_query, new_key, new_value, step_decay, norm_gain
):
    seqs, span, width = tokens.shape
    heads = key_weight.shape[1] // HEAD_DIM
    n_sp = lax.axis_size("sp")
    token_rows = tokens.reshape(seqs * span, width)
    decays = log_decay.reshape(heads * seqs, span)
    totals = jnp.sum(decays, axis=-1)
    totals = jnp.broadcast_to(jnp.pad(totals, (0, 128 - heads * seqs))[None, :], (8, 128))
    start = (lax.axis_index("sp") // 2) * (2 * span)
    positions = (start + jnp.arange(2 * span, dtype=jnp.int32)).astype(jnp.float32)
    half = HEAD_DIM // 2
    inverse = 10000.0 ** (-jnp.arange(half, dtype=jnp.float32) * (2.0 / HEAD_DIM))
    angles = positions[:, None] * inverse[None, :]
    cosine = jnp.cos(angles) * HEAD_DIM ** (-0.5)
    sine = jnp.sin(angles) * HEAD_DIM ** (-0.5)
    cos = jnp.concatenate([cosine] * 4, axis=-1)
    sin = jnp.concatenate([-sine, sine] * 2, axis=-1)
    summed = prompt_states(
        token_rows, key_weight, value_weight, decays, totals, cos, sin, seqs, span, heads, n_sp
    )
    summed = summed.astype(F32).reshape(seqs * HEAD_DIM, heads, HEAD_DIM)
    end_pos = jnp.full((seqs, heads), float(span * n_sp), jnp.float32)
    query = rotate_half(new_query.astype(jnp.float32).reshape(seqs, heads, HEAD_DIM), end_pos)
    key_new = rotate_half(
        new_key.astype(jnp.float32).reshape(seqs, heads, HEAD_DIM), end_pos
    ) * HEAD_DIM ** (-0.5)
    value_new = new_value.astype(jnp.float32).reshape(seqs, heads, HEAD_DIM)
    decay_all = jnp.repeat(jnp.exp(step_decay).T, HEAD_DIM, axis=0)
    key_all = jnp.transpose(key_new, (0, 2, 1)).reshape(seqs * HEAD_DIM, heads)
    value_all = jnp.repeat(value_new, HEAD_DIM, axis=0)
    state_cache = decay_all[:, :, None] * summed + key_all[:, :, None] * value_all
    state_seq = state_cache.reshape(seqs, HEAD_DIM, heads, HEAD_DIM)
    raw = jnp.einsum("sha,sahb->shb", query, state_seq, precision=lax.Precision.HIGHEST)
    center = jnp.mean(raw, axis=-1, keepdims=True)
    spread = jnp.mean(jnp.square(raw - center), axis=-1, keepdims=True)
    normed = (raw - center) * lax.rsqrt(spread + 1e-06) * norm_gain.reshape(heads, HEAD_DIM)
    first_read = normed.reshape(seqs, heads * HEAD_DIM).astype(jnp.bfloat16)
    return (state_cache, first_read)


def solution(mesh):
    placed = (
        P("gr", "sp", None),
        P("sp", "tp"),
        P("sp", "tp"),
        P("tp", "gr", "sp"),
        P("gr", "tp"),
        P("gr", "tp"),
        P("gr", "tp"),
        P("tp", "gr"),
        P("tp"),
    )
    return jax.shard_map(
        shards,
        mesh=mesh,
        in_specs=placed,
        out_specs=(P("gr", "tp", None), P("gr", "tp")),
        check_vma=False,
    )
```

time: 379 us -> 134 us (0.35)
  waiting for transfers between devices: 288 us -> 0 us
  Pallas kernels: 0 us -> 120 us
  blocking collectives: 28.8 us -> 0 us
  matrix products: 24.7 us -> 2.25 us
  between operations: 14 us -> 0.82 us
  local copies, waits for them, and re-layouts: 16 us -> 6.9 us
    all_gather x2 -> x0, waiting for transfers between devices: 214 us -> none  [the longest x1 116 us: shards(): lax.all_gather(value_weight, 'sp', axis=0, tiled=True)]
    pallas_call x0 -> x1, Pallas kernels: none -> 120 us  [prompt_states(): pl.pallas_call(functools.partial(kernel, (n_sp, seqs, span, heads)), out_...]
    psum x1 -> x0, waiting for transfers between devices: 73.2 us -> none  [shards(): summed = lax.psum(term, 'sp')]
    all_gather x1 -> x0, blocking collectives: 28.8 us -> none  [entering(): everything = lax.all_gather(x, axis)]
    dot_general x3 -> x0, matrix products: 21.3 us -> none  [the longest x1 10.1 us: shards(): jnp.dot(token_rows, whole_values, preferred_element_type=jnp.float32)]
    reshape x8 -> x4, local copies, waits for them, and re-layouts: 10.8 us -> 1.48 us  [the longest x1 0.77 us: shards(): value_new = new_value.astype(jnp.float32).reshape(seqs, heads, HEAD_DIM)]
  transfers between devices with their start and end apart: 3 -> 0, of which waited for: 3 -> 0; matrix products, arithmetic and copies ran while one was open for 4% -> 0% of each run, Pallas kernels for 0% -> 0%
where the time goes in v1:
time: 134 us
  Pallas kernels  120 us (90%)
  local copies, waits for them, and re-layouts  6.9 us (5%)
  other arithmetic  4.13 us (3%)
  matrix products  2.25 us (2%)
    pallas_call x1, Pallas kernels, prompt_states(): pl.pallas_call(functools.partial(kernel, (n_sp, seqs, span, heads)), out_...  120 us

profile of v1, /device:TPU:0, one launch (start us, length us, event | category | flops | bytes accessed | tf_op | source)
XLA Modules:
  0.0 133.7 jit_solution(6460958033788072298)
XLA Ops:
  0.6 0.8 reshape.92
  1.4 0.1 broadcast_in_dim.8
  1.6 0.0 copy-start.2
  1.6 2.0 %copy.30 = f32[256,16,64]{0,2,1:T(8,128)} copy(f32[256,16,64]{2,1,0:T(8,128)S(1)} %bitcast.18) | data formatting | bytes 2097152 | tf_op jit(solution)/shard_map/reshape | solution.py:435
  3.6 0.1 reduce_sum.29
  3.7 0.1 reduce_sum.30
  3.8 0.6 broadcast_in_dim.7.tot
  4.4 0.5 fusion.4
  4.9 1.0 pad_maximum_fusion
  5.9 119.6 %shard_map.104 = bf16[256,1024]{1,0:T(8,128)(2,1)} custom-call(bf16[512,4096]{1,0:T(8,128)(2,1)} %bitcast.20, bf16[512,1024]{1,0:T(8,128)(2,1)} %kw.1, bf16[512,1024]{1,0:T(8,128)(2,1)} %vw.1, f32[64,128]{1,0:T(8,128)} %bitcast.24, f32[8,128]{1,0:T(8,128)} %broadcast_in_dim.7.tot, f32[256,128]{1,0:T(8,128)} %get-tuple-element.11.cos_ref, ...), custom_call_target="tpu_custom_call" | custom-call | tf_op jit(solution)/shard_map/pallas_call | solution.py:364
  125.5 0.0 copy-start.1
  125.5 1.3 copy.23
  126.9 0.1 reshape.94
  127.0 0.1 multiply_cosine_fusion.1
  127.1 0.1 reshape.90
  127.2 0.1 multiply_subtract_fusion
  127.2 0.1 fusion.5
  127.4 0.1 mul.169
  127.5 0.1 copy.21
  127.5 0.1 broadcast_in_dim.6
  127.6 0.1 mul.151
  127.7 1.2 multiply_add_fusion.1
  128.9 0.5 reshape.88
  129.4 0.1 copy.26
  129.5 0.7 multiply_add_fusion
  130.3 0.0 copy-start.5
  130.3 2.3 %fusion = f32[4,16,1,64]{3,2,1,0:T(1,128)S(1)} fusion(f32[4,16,64,1]{2,3,1,0:T(1,128)S(1)} %bitcast.25, f32[4,64,16,64]{3,2,1,0:T(8,128)S(1)} %multiply_add_fusion), kind=kOutput, calls=%fused_computation | convolution fusion | flops 3145728 | bytes 1081344 | tf_op jit(solution)/shard_map/sha,sahb->shb/dot_general | solution.py:438
  132.5 0.1 mul.182
  132.6 0.1 reduce_sum.31
  132.7 0.2 multiply_reduce_fusion
  132.9 0.1 multiply_convert_fusion
  133.0 0.7 convert_element_type.24
  (19 shorter events, 0.1 us)
Async XLA Ops:
  1.6 2.0 %copy-start.2 = (f32[16,4,128]{2,1,0:T(4,128)S(1)}, f32[16,4,128]{2,1,0:T(4,128)}, u32[]{:S(2)}) copy-start(f32[16,4,128]{2,1,0:T(4,128)} %param.12) | copy-start | bytes 98308
  5.9 121.0 %copy-start.3 = (bf16[4,1024]{1,0:T(4,128)(2,1)S(1)}, bf16[4,1024]{1,0:T(4,128)(2,1)}, u32[]{:S(2)}) copy-start(bf16[4,1024]{1,0:T(4,128)(2,1)} %param.13) | copy-start | bytes 24580
  5.9 121.2 %copy-start.4 = (bf16[4,1024]{1,0:T(4,128)(2,1)S(1)}, bf16[4,1024]{1,0:T(4,128)(2,1)}, u32[]{:S(2)}) copy-start(bf16[4,1024]{1,0:T(4,128)(2,1)} %param.14) | copy-start | bytes 24580
  125.5 2.0 %copy-start.6 = (f32[16,4]{0,1:T(4,128)S(1)}, f32[16,4]{0,1:T(4,128)}, u32[]{:S(2)}) copy-start(f32[16,4]{0,1:T(4,128)} %param.16) | copy-start | bytes 772
  125.5 2.2 %copy-start.1 = (f32[256,16,64]{0,2,1:T(8,128)S(1)}, f32[256,16,64]{0,2,1:T(8,128)}, u32[]{:S(2)}) copy-start(f32[256,16,64]{0,2,1:T(8,128)} %copy.30) | copy-start | bytes 3145732
  126.8 2.0 %copy-start = (bf16[256,1024]{1,0:T(8,128)(2,1)S(1)}, bf16[256,1024]{1,0:T(8,128)(2,1)}, u32[]{:S(2)}) copy-start(bf16[256,1024]{1,0:T(8,128)(2,1)} %shard_map.104) | copy-start | bytes 1572868
  130.3 2.3 %copy-start.5 = (f32[1024]{0:T(1024)S(1)}, f32[1024]{0:T(1024)}, u32[]{:S(2)}) copy-start(f32[1024]{0:T(1024)} %param.17) | copy-start | bytes 12292

commit v2 on v1

--- a/solution.py
+++ b/solution.py
@@ -2,13 +2,14 @@
 
 import jax
 import jax.numpy as jnp
+import numpy as np
 from jax import lax
 from jax.experimental import pallas as pl
 from jax.experimental.pallas import tpu as pltpu
 from jax.sharding import PartitionSpec as P
 
 HEAD_DIM = 64
-SUB = 2
+SUB = 4
 MESH = pl.DeviceIdType.MESH
 F32 = jnp.float32
 HIGH = lax.Precision.HIGHEST
@@ -16,9 +17,9 @@
 
 def kernel(
     sizes,
-    tok, kw, vw, ld, tot, cos_ref, sin_ref,
-    out,
-    toks, w, keys, vals, lds, tots, part, got, full,
+    tok, kw, vw, ld, cos_tab, sin_tab, nq, nk, nv, sd, gain,
+    out, read,
+    toks, w, kv, acc, lds, tots, part, got, full, cos_ref, sin_ref, ends, qx, outer, decay,
     l_sem, tok_s, tok_r, core_s, core_r, yw_s, yw_r, up_s, dn_s, z_r, x_s, x_r,
     ld_s, ld_r, tot_s, tot_r, rs_s, rs_r, ag_s, ag_r, yg_s, yg_r,
 ):
@@ -52,7 +53,10 @@
         pltpu.make_async_copy(vw.at[:, mine(b)], w.at[1, shard_rows(sp)], l_sem.at[1]),
         pltpu.make_async_copy(tok, toks.at[b], l_sem.at[2]),
         pltpu.make_async_copy(ld, lds.at[b], l_sem.at[3]),
-        pltpu.make_async_copy(tot, tots.at[sp], l_sem.at[4]),
+        pltpu.make_async_copy(cos_tab.at[pl.ds(pl.multiple_of(a * 2 * span, 8), 2 * span)], cos_ref, l_sem.at[4]),
+        pltpu.make_async_copy(sin_tab.at[pl.ds(pl.multiple_of(a * 2 * span, 8), 2 * span)], sin_ref, l_sem.at[5]),
+        pltpu.make_async_copy(cos_tab.at[pl.ds(n_sp * span, 8)], ends.at[0], l_sem.at[6]),
+        pltpu.make_async_copy(sin_tab.at[pl.ds(n_sp * span, 8)], ends.at[1], l_sem.at[7]),
     ]
     for c in local:
         c.start()
@@ -117,48 +121,124 @@
 
     for q in range(SUB):
         launch(sp, q)
-    local[4].wait()
 
     def tsend(k):
         return remote(tots.at[sp], tots.at[sp], tot_s.at[k], tot_r.at[k], (g, lax.rem(sp + k, n_sp), tp))
 
-    @pl.loop(1, n_sp)
-    def _(k):
-        tsend(k).start()
-
+    for c in local[2:]:
+        c.wait()
+    tots[sp] = jnp.zeros(tots.shape[1:], F32)
+    tots[sp, :, 0:hs] = lax.dot_general(
+        jnp.ones((8, span), F32), lds[b], (((1,), (1,)), ((), ())), precision=HIGH, preferred_element_type=F32
+    )
+
+    lanes = lax.broadcasted_iota(jnp.int32, (HEAD_DIM, 128), 1)
+    subs = lax.broadcasted_iota(jnp.int32, (HEAD_DIM, 128), 0)
+    diagonal = lanes % HEAD_DIM == subs
+    same_head = jnp.where(
+        lax.broadcasted_iota(jnp.int32, (128, 128), 0) // HEAD_DIM
+        == lax.broadcasted_iota(jnp.int32, (128, 128), 1) // HEAD_DIM, 1.0, 0.0
+    ).astype(F32)
+
+    def exact(x, y):
+        return jnp.dot(x, y, precision=HIGH, preferred_element_type=F32)
+
+    def at_end(u):
+        low = lax.broadcasted_iota(jnp.int32, u.shape, 1) % HEAD_DIM < HEAD_DIM // 2
+        turned = jnp.where(low, pltpu.roll(u, 128 - 32, 1), pltpu.roll(u, 32, 1))
+        return u * ends[0, 0:1, :] + turned * ends[1, 0:1, :]
+
+    head_lane = lax.broadcasted_iota(jnp.int32, (heads, 2 * cols), 1) // HEAD_DIM
+    head_row = lax.broadcasted_iota(jnp.int32, (heads, 2 * cols), 0)
+    spread_heads = jnp.where(head_lane == head_row, 1.0, 0.0).astype(F32)
+    decay[...] = jnp.exp(exact(sd[...], spread_heads))
+
+    def new_token(c0):
+        chunk = pl.ds(c0, 128)
+        query = at_end(nq[:, chunk].astype(F32)) * HEAD_DIM ** 0.5
+        key_new = at_end(nk[:, chunk].astype(F32))
+        value_new = nv[:, chunk].astype(F32)
+        for s in range(seqs):
+            at = pl.ds(s * HEAD_DIM, HEAD_DIM)
+            qx[at, chunk] = exact(jnp.where(diagonal, query[s:s + 1], 0.0), same_head)
+            column = exact(jnp.where(diagonal, key_new[s:s + 1], 0.0), same_head)
+            outer[at, chunk] = column * value_new[s:s + 1]
+
+    def zstep(d, bb, q):
+        below = (a - d) * 2 + (b if bb == 0 else ob)
+        above = (a + d) * 2 + (b if bb == 0 else ob)
+
+        @pl.when(a - d >= 0)
+        def _():
+            zsend(below, q, True).wait_recv()
+
+            @pl.when(a < n_a - 1)
+            def _():
+                zsend(below, q, True).start()
+
+            xsend(below, q).start()
+
+        @pl.when(a + d < n_a)
+        def _():
+            zsend(above, q, False).wait_recv()
+
+            @pl.when(a > 0)
+            def _():
+                zsend(above, q, False).start()
+
+            xsend(above, q).start()
+
+    chunks = list(range(0, 2 * cols, 128))
     for q in range(SUB):
         for m in range(2):
             @pl.when(g == m)
             def _():
                 yw(m, q).wait_recv()
         launch(a * 2 + ob, q)
-
-    @pl.loop(1, n_a)
+        zstep(1, 0, q)
+        for c0 in chunks[q::SUB]:
+            new_token(c0)
+
+    @pl.loop(1, n_sp)
+    def _(k):
+        tsend(k).start()
+
+    tile = min(256, rows)
+
+    def own_product(m, s, fresh=False):
+        depth_at = shard_rows(s)
+
+        @pl.loop(0, rows // tile)
+        def _(r):
+            at = pl.ds(pl.multiple_of(r * tile, tile), tile)
+            new = jnp.dot(toks[b, at, depth_at], w[m, depth_at, :], preferred_element_type=F32)
+            acc[m, at, :] = new if fresh else acc[m, at, :] + new
+
+    own_product(0, sp, True)
+    own_product(1, sp, True)
+    own_product(g, a * 2 + ob)
+
+    def take(d, bb, mats):
+        side = b if bb == 0 else ob
+        for inside, s in ((a - d >= 0, (a - d) * 2 + side), (a + d < n_a, (a + d) * 2 + side)):
+            @pl.when(inside)
+            def _():
+                if 0 in mats:
+                    own_product(g, s)
+                if 1 in mats:
+                    for q in range(SUB):
+                        xrecv(s, q).wait_recv()
+                    own_product(1 - g, s)
+
+    for q in range(SUB):
+        zstep(1, 1, q)
+
+    @pl.loop(2, n_a)
     def _(d):
         for bb in range(2):
             for q in range(SUB):
-                below = (a - d) * 2 + (b if bb == 0 else ob)
-                above = (a + d) * 2 + (b if bb == 0 else ob)
-
-                @pl.when(a - d >= 0)
-                def _():
-                    zsend(below, q, True).wait_recv()
-
-                    @pl.when(a < n_a - 1)
-                    def _():
-                        zsend(below, q, True).start()
-
-                    xsend(below, q).start()
-
-                @pl.when(a + d < n_a)
-                def _():
-                    zsend(above, q, False).wait_recv()
-
-                    @pl.when(a > 0)
-                    def _():
-                        zsend(above, q, False).start()
-
-                    xsend(above, q).start()
+                zstep(d, bb, q)
+            take(d - 1, bb, (0, 1))
 
     ytok_in = remote(toks.at[ob, half_rows], toks.at[ob, half_rows], tok_s, tok_r, y_peer)
     ctok = remote(toks.at[ob, half_rows], toks.at[ob, half_rows], core_s, core_r, core_peer)
@@ -169,9 +249,6 @@
     @pl.loop(1, n_sp)
     def _(k):
         tsend(k).wait_recv()
-
-    for c in local[2:4]:
-        c.wait()
 
     pos_t = lax.broadcasted_iota(jnp.int32, (span, span), 0)
     pos_u = lax.broadcasted_iota(jnp.int32, (span, span), 1)
@@ -191,34 +268,27 @@
     row_hs = lax.broadcasted_iota(jnp.int32, (hs, cols), 0)
     lane_head = lax.broadcasted_iota(jnp.int32, (hs, cols), 1) // HEAD_DIM + b * (heads // 2)
 
+    def partner_product(m):
+        @pl.loop(0, rows // tile)
+        def _(r):
+            at = pl.ds(pl.multiple_of(r * tile, tile), tile)
+            new = jnp.dot(toks[ob, at, :], w[m], preferred_element_type=F32)
+            kv[m, ob, at, :] = new.astype(jnp.bfloat16)
+            kv[m, b, at, :] = acc[m, at, :].astype(jnp.bfloat16)
+
+    for bb in range(2):
+        take(n_a - 1, bb, (0,))
     ctok.wait_recv()
-
-    @pl.loop(1, n_a)
-    def _(d):
-        for bb in range(2):
-            for q in range(SUB):
-                @pl.when(a - d >= 0)
-                def _():
-                    xrecv((a - d) * 2 + (b if bb == 0 else ob), q).wait_recv()
-
-                @pl.when(a + d < n_a)
-                def _():
-                    xrecv((a + d) * 2 + (b if bb == 0 else ob), q).wait_recv()
-
+    partner_product(g)
     for q in range(SUB):
         for m in range(2):
             @pl.when(g == m)
             def _():
                 yw(1 - m, q).wait_recv()
-
-    tile = min(256, rows)
-    for tb in range(2):
-        @pl.loop(0, rows // tile)
-        def _(r):
-            at = pl.ds(pl.multiple_of(r * tile, tile), tile)
-            lhs = toks[tb, at, :]
-            keys[tb, at, :] = jnp.dot(lhs, w[0], preferred_element_type=F32).astype(jnp.bfloat16)
-            vals[tb, at, :] = jnp.dot(lhs, w[1], preferred_element_type=F32).astype(jnp.bfloat16)
+    own_product(1 - g, a * 2 + ob)
+    for bb in range(2):
+        take(n_a - 1, bb, (1,))
+    partner_product(1 - g)
 
     lane = lax.broadcasted_iota(jnp.int32, (span, 128), 1)
     first = lane % HEAD_DIM < HEAD_DIM // 2
@@ -234,13 +304,13 @@
             total = None
             for tb in range(2):
                 at = pl.ds(s * span, span)
-                u = keys[tb, at, pl.ds(c0, 128)].astype(F32)
+                u = kv[0, tb, at, pl.ds(c0, 128)].astype(F32)
                 turned = jnp.where(first, pltpu.roll(u, 128 - 32, 1), pltpu.roll(u, 32, 1))
                 spot = pl.ds(tb * span, span)
                 rk = u * cos_ref[spot, :] + turned * sin_ref[spot, :]
                 weighted = (rk * weights[tb][:, c0:c0 + 128]).astype(jnp.bfloat16)
                 term = lax.dot_general(
-                    weighted, vals[tb, at, pl.ds(c0, 128)], (((0,), (0,)), ((), ())),
+                    weighted, kv[1, tb, at, pl.ds(c0, 128)], (((0,), (0,)), ((), ())),
                     preferred_element_type=F32,
                 )
                 total = term if total is None else total + term
@@ -295,8 +365,21 @@
     def _(k):
         yg(k, ob).wait_recv()
 
-    out[:, 0:cols] = full[0]
-    out[:, cols:2 * cols] = full[1]
+    for c0 in range(0, 2 * cols, 128):
+        chunk = pl.ds(c0, 128)
+        raws, states = [], []
+        for s in range(seqs):
+            at = pl.ds(s * HEAD_DIM, HEAD_DIM)
+            summed = full[c0 // cols, at, pl.ds(c0 % cols, 128)].astype(F32)
+            state = decay[s:s + 1, chunk] * summed + outer[at, chunk]
+            raws.append(jnp.sum(qx[at, chunk] * state, axis=0, keepdims=True))
+            states.append(state)
+        out[chunk, :] = jnp.concatenate(states, axis=0).T
+        raw = jnp.concatenate(raws, axis=0)
+        center = exact(raw, same_head) * (1.0 / HEAD_DIM)
+        off = raw - center
+        spread = exact(off * off, same_head) * (1.0 / HEAD_DIM)
+        read[:, chunk] = (off * lax.rsqrt(spread + 1e-06) * gain[:, chunk]).astype(jnp.bfloat16)
 
     @pl.loop(0, n_a)
     def _(k):
@@ -350,7 +433,7 @@
                     xsend(above, q).wait_send()
 
 
-def prompt_states(token_rows, key_weight, value_weight, decays, totals, cos, sin, seqs, span, heads, n_sp):
+def prompt_states(token_rows, key_weight, value_weight, decays, cos, sin, step, seqs, span, heads, n_sp):
     rows, width = token_rows.shape
     depth, whole = key_weight.shape
     cols = whole // 2
@@ -363,20 +446,29 @@
     vmem = pl.BlockSpec(memory_space=pltpu.VMEM)
     return pl.pallas_call(
         functools.partial(kernel, (n_sp, seqs, span, heads)),
-        out_shape=jax.ShapeDtypeStruct((state_rows, whole), bf16),
-        in_specs=[hbm, hbm, hbm, hbm, hbm, vmem, vmem],
-        out_specs=vmem,
+        out_shape=(
+            jax.ShapeDtypeStruct((whole, state_rows), F32),
+            jax.ShapeDtypeStruct((seqs, whole), bf16),
+        ),
+        in_specs=[hbm] * 6 + [vmem] * 5,
+        out_specs=(vmem, vmem),
         scratch_shapes=[
             pltpu.VMEM((2, rows, width), bf16),
             pltpu.VMEM((2, n_sp * depth, cols), bf16),
-            pltpu.VMEM((2, rows, cols), bf16),
-            pltpu.VMEM((2, rows, cols), bf16),
+            pltpu.VMEM((2, 2, rows, cols), bf16),
+            pltpu.VMEM((2, rows, cols), F32),
             pltpu.VMEM((2, hs, span), F32),
             pltpu.VMEM((n_sp, 8, 128), F32),
             pltpu.VMEM((state_rows, cols), bf16),
             pltpu.VMEM((n_a, state_rows // n_a, cols), bf16),
             pltpu.VMEM((2, state_rows, cols), bf16),
-            dma((5,)), dma, dma, dma, dma,
+            pltpu.VMEM((2 * span, 128), F32),
+            pltpu.VMEM((2 * span, 128), F32),
+            pltpu.VMEM((2, 8, 128), F32),
+            pltpu.VMEM((state_rows, whole), F32),
+            pltpu.VMEM((state_rows, whole), F32),
+            pltpu.VMEM((seqs, whole), F32),
+            dma((8,)), dma, dma, dma, dma,
             dma((2, SUB)), dma((2, SUB)),
             dma((n_sp, SUB)), dma((n_sp, SUB)), dma((n_sp, SUB)),
             dma((n_sp, SUB)), dma((n_sp, SUB)),
@@ -386,19 +478,18 @@
         compiler_params=pltpu.CompilerParams(
             collective_id=0, has_side_effects=True, vmem_limit_bytes=56 * 1024 * 1024
         ),
-    )(token_rows, key_weight, value_weight, decays, totals, cos, sin)
-
-
-def rotate_half(values, positions):
-    half = values.shape[-1] // 2
-    inverse = 10000.0 ** (-jnp.arange(half, dtype=jnp.float32) * (2.0 / values.shape[-1]))
-    angles = positions[..., None] * inverse
-    cosine = jnp.cos(angles)
-    sine = jnp.sin(angles)
-    first, second = (values[..., :half], values[..., half:])
-    return jnp.concatenate(
-        [first * cosine - second * sine, second * cosine + first * sine], axis=-1
-    )
+    )(token_rows, key_weight, value_weight, decays, cos, sin, *step)
+
+
+def position_tables(length):
+    half = HEAD_DIM // 2
+    inverse = np.float32(10000.0) ** (-np.arange(half, dtype=np.float32) * np.float32(2.0 / HEAD_DIM))
+    angles = np.arange(length + 8, dtype=np.float32)[:, None] * inverse[None, :].astype(np.float32)
+    cosine = np.cos(angles.astype(np.float64)) * HEAD_DIM ** -0.5
+    sine = np.sin(angles.astype(np.float64)) * HEAD_DIM ** -0.5
+    cos = np.concatenate([cosine] * 4, axis=-1).astype(np.float32)
+    sin = np.concatenate([-sine, sine] * 2, axis=-1).astype(np.float32)
+    return cos, sin
 
 
 def shards(
@@ -409,38 +500,13 @@
     n_sp = lax.axis_size("sp")
     token_rows = tokens.reshape(seqs * span, width)
     decays = log_decay.reshape(heads * seqs, span)
-    totals = jnp.sum(decays, axis=-1)
-    totals = jnp.broadcast_to(jnp.pad(totals, (0, 128 - heads * seqs))[None, :], (8, 128))
-    start = (lax.axis_index("sp") // 2) * (2 * span)
-    positions = (start + jnp.arange(2 * span, dtype=jnp.int32)).astype(jnp.float32)
-    half = HEAD_DIM // 2
-    inverse = 10000.0 ** (-jnp.arange(half, dtype=jnp.float32) * (2.0 / HEAD_DIM))
-    angles = positions[:, None] * inverse[None, :]
-    cosine = jnp.cos(angles) * HEAD_DIM ** (-0.5)
-    sine = jnp.sin(angles) * HEAD_DIM ** (-0.5)
-    cos = jnp.concatenate([cosine] * 4, axis=-1)
-    sin = jnp.concatenate([-sine, sine] * 2, axis=-1)
-    summed = prompt_states(
-        token_rows, key_weight, value_weight, decays, totals, cos, sin, seqs, span, heads, n_sp
+    cos, sin = position_tables(span * n_sp)
+    step = (new_query, new_key, new_value, step_decay.T, norm_gain.reshape(1, -1))
+    state, read = prompt_states(
+        token_rows, key_weight, value_weight, decays, jnp.asarray(cos), jnp.asarray(sin), step,
+        seqs, span, heads, n_sp,
     )
-    summed = summed.astype(F32).reshape(seqs * HEAD_DIM, heads, HEAD_DIM)
-    end_pos = jnp.full((seqs, heads), float(span * n_sp), jnp.float32)
-    query = rotate_half(new_query.astype(jnp.float32).reshape(seqs, heads, HEAD_DIM), end_pos)
-    key_new = rotate_half(
-        new_key.astype(jnp.float32).reshape(seqs, heads, HEAD_DIM), end_pos
-    ) * HEAD_DIM ** (-0.5)
-    value_new = new_value.astype(jnp.float32).reshape(seqs, heads, HEAD_DIM)
-    decay_all = jnp.repeat(jnp.exp(step_decay).T, HEAD_DIM, axis=0)
-    key_all = jnp.transpose(key_new, (0, 2, 1)).reshape(seqs * HEAD_DIM, heads)
-    value_all = jnp.repeat(value_new, HEAD_DIM, axis=0)
-    state_cache = decay_all[:, :, None] * summed + key_all[:, :, None] * value_all
-    state_seq = state_cache.reshape(seqs, HEAD_DIM, heads, HEAD_DIM)
-    raw = jnp.einsum("sha,sahb->shb", query, state_seq, precision=lax.Precision.HIGHEST)
-    center = jnp.mean(raw, axis=-1, keepdims=True)
-    spread = jnp.mean(jnp.square(raw - center), axis=-1, keepdims=True)
-    normed = (raw - center) * lax.rsqrt(spread + 1e-06) * norm_gain.reshape(heads, HEAD_DIM)
-    first_read = normed.reshape(seqs, heads * HEAD_DIM).astype(jnp.bfloat16)
-    return (state_cache, first_read)
+    return (state.T.reshape(seqs * HEAD_DIM, heads, HEAD_DIM), read)
 
 
 def solution(mesh):

time: 134 us -> 117 us (0.87)
  Pallas kernels: 120 us -> 113 us
  other arithmetic: 4.13 us -> 0 us
  local copies, waits for them, and re-layouts: 6.9 us -> 3.59 us
  matrix products: 2.25 us -> 0 us
    pallas_call x1, Pallas kernels: 120 us -> 113 us  [prompt_states(): pl.pallas_call(functools.partial(kernel, (n_sp, seqs, span, heads)), out_...]
    unnamed x14 -> x2, local copies, waits for them, and re-layouts: 0.04 us -> 3.59 us
    reshape x5 -> x0, local copies, waits for them, and re-layouts: 3.47 us -> none  [the longest x1 1.99 us: shards(): value_all = jnp.repeat(value_new, HEAD_DIM, axis=0)]
    dot_general x1 -> x0, matrix products: 2.25 us -> none  [shards(): jnp.einsum('sha,sahb->shb', query, state_seq, precision=lax.Precision.HIG...]
    convert_element_type x2 -> x0, local copies, waits for them, and re-layouts: 2.02 us -> none  [the longest x1 1.33 us: shards(): summed = summed.astype(F32).reshape(seqs * HEAD_DIM, heads, HEAD_DIM)]
    add x2 -> x0, other arithmetic: 1.88 us -> none  [shards(): decay_all[:, :, None] * summed + key_all[:, :, None] * value_all]
where the time goes in v2:
time: 117 us
  Pallas kernels  113 us (97%)
  local copies, waits for them, and re-layouts  3.59 us (3%)
    pallas_call x1, Pallas kernels, prompt_states(): pl.pallas_call(functools.partial(kernel, (n_sp, seqs, span, heads)), out_...  113 us
    unnamed x2, local copies, waits for them, and re-layouts  3.59 us

profile of v2, /device:TPU:0, one launch (start us, length us, event | category | flops | bytes accessed | tf_op | source)
XLA Modules:
  0.0 117.0 jit_solution(12320822414564129487)
XLA Ops:
  0.6 112.7 %shard_map.122 = (f32[1024,256]{1,0:T(8,128)}, bf16[4,1024]{1,0:T(4,128)(2,1)}) custom-call(bf16[512,4096]{1,0:T(8,128)(2,1)} %bitcast.7, bf16[512,1024]{1,0:T(8,128)(2,1)} %kw.1, bf16[512,1024]{1,0:T(8,128)(2,1)} %vw.1, f32[64,128]{1,0:T(8,128)} %bitcast.9, f32[1032,128]{1,0:T(8,128)} %constant.4.clone.cos_tab, f32[1032,128]{1,0:T(8,128)} %constant.5.clone.sin_tab, ...), custom_call_target="tpu_custom_call" | custom-call | tf_op jit(solution)/shard_map/pallas_call | solution.py:447
  113.4 2.3 %copy.15 = f32[256,16,64]{0,2,1:T(8,128)} copy(f32[256,16,64]{0,2,1:T(8,128)} %bitcast.8) | data formatting | bytes 2097152
  115.7 1.3 %copy.16 = bf16[4,1024]{1,0:T(4,128)(2,1)} copy(bf16[4,1024]{1,0:T(4,128)(2,1)} %get-tuple-element.9) | data formatting | bytes 16384

commit v3 on v2

--- a/solution.py
+++ b/solution.py
@@ -19,7 +19,7 @@
     sizes,
     tok, kw, vw, ld, cos_tab, sin_tab, nq, nk, nv, sd, gain,
     out, read,
-    toks, w, kv, acc, lds, tots, part, got, full, cos_ref, sin_ref, ends, qx, outer, decay,
+    toks, w, kv, acc, lds, tots, part, got, full, cos_ref, sin_ref, ends, qx, outer, decay, wts,
     l_sem, tok_s, tok_r, core_s, core_r, yw_s, yw_r, up_s, dn_s, z_r, x_s, x_r,
     ld_s, ld_r, tot_s, tot_r, rs_s, rs_r, ag_s, ag_r, yg_s, yg_r,
 ):
@@ -233,7 +233,7 @@
     for q in range(SUB):
         zstep(1, 1, q)
 
-    @pl.loop(2, n_a)
+    @pl.loop(2, n_a - 1)
     def _(d):
         for bb in range(2):
             for q in range(SUB):
@@ -242,8 +242,6 @@
 
     ytok_in = remote(toks.at[ob, half_rows], toks.at[ob, half_rows], tok_s, tok_r, y_peer)
     ctok = remote(toks.at[ob, half_rows], toks.at[ob, half_rows], core_s, core_r, core_peer)
-    ytok_in.wait_recv()
-    ctok.start()
     yld.wait_recv()
 
     @pl.loop(1, n_sp)
@@ -268,6 +266,23 @@
     row_hs = lax.broadcasted_iota(jnp.int32, (hs, cols), 0)
     lane_head = lax.broadcasted_iota(jnp.int32, (hs, cols), 1) // HEAD_DIM + b * (heads // 2)
 
+    def prompt_weights(s):
+        select = jnp.where(row_hs == lane_head * seqs + s, 1.0, 0.0).astype(F32)
+        for tb in range(2):
+            wts[tb, pl.ds(s * span, span), :] = jnp.exp(exact(suffix[tb], select))
+
+    for q in range(SUB):
+        zstep(n_a - 1, 0, q)
+        for s in range(q, seqs, SUB):
+            prompt_weights(s)
+    take(n_a - 2, 0, (0, 1))
+    for q in range(SUB):
+        zstep(n_a - 1, 1, q)
+        if q == SUB // 2 - 1:
+            ytok_in.wait_recv()
+            ctok.start()
+    take(n_a - 2, 1, (0, 1))
+
     def partner_product(m):
         @pl.loop(0, rows // tile)
         def _(r):
@@ -295,11 +310,6 @@
     lane_out = lax.broadcasted_iota(jnp.int32, (HEAD_DIM, 128), 1)
     block = seqs * HEAD_DIM // n_a
     for s in range(seqs):
-        select = jnp.where(row_hs == lane_head * seqs + s, 1.0, 0.0).astype(F32)
-        weights = [
-            jnp.exp(jnp.dot(suffix[tb], select, precision=HIGH, preferred_element_type=F32))
-            for tb in range(2)
-        ]
         for c0 in range(0, cols, 128):
             total = None
             for tb in range(2):
@@ -308,7 +318,7 @@
                 turned = jnp.where(first, pltpu.roll(u, 128 - 32, 1), pltpu.roll(u, 32, 1))
                 spot = pl.ds(tb * span, span)
                 rk = u * cos_ref[spot, :] + turned * sin_ref[spot, :]
-                weighted = (rk * weights[tb][:, c0:c0 + 128]).astype(jnp.bfloat16)
+                weighted = (rk * wts[tb, at, pl.ds(c0, 128)]).astype(jnp.bfloat16)
                 term = lax.dot_general(
                     weighted, kv[1, tb, at, pl.ds(c0, 128)], (((0,), (0,)), ((), ())),
                     preferred_element_type=F32,
@@ -468,6 +478,7 @@
             pltpu.VMEM((state_rows, whole), F32),
             pltpu.VMEM((state_rows, whole), F32),
             pltpu.VMEM((seqs, whole), F32),
+            pltpu.VMEM((2, rows, cols), F32),
             dma((8,)), dma, dma, dma, dma,
             dma((2, SUB)), dma((2, SUB)),
             dma((n_sp, SUB)), dma((n_sp, SUB)), dma((n_sp, SUB)),

time: 117 us -> 132 us (1.13)
  Pallas kernels: 113 us -> 128 us
    pallas_call x1, Pallas kernels: 113 us -> 128 us  [prompt_states(): pl.pallas_call(functools.partial(kernel, (n_sp, seqs, span, heads)), out_...]
where the time goes in v3:
time: 132 us
  Pallas kernels  128 us (97%)
  local copies, waits for them, and re-layouts  3.59 us (3%)
    pallas_call x1, Pallas kernels, prompt_states(): pl.pallas_call(functools.partial(kernel, (n_sp, seqs, span, heads)), out_...  128 us
    unnamed x2, local copies, waits for them, and re-layouts  3.59 us

profile of v3, /device:TPU:0, one launch (start us, length us, event | category | flops | bytes accessed | tf_op | source)
XLA Modules:
  0.0 131.9 jit_solution(16194978438611112824)
XLA Ops:
  0.6 127.6 %shard_map.122 = (f32[1024,256]{1,0:T(8,128)}, bf16[4,1024]{1,0:T(4,128)(2,1)}) custom-call(bf16[512,4096]{1,0:T(8,128)(2,1)} %bitcast.7, bf16[512,1024]{1,0:T(8,128)(2,1)} %kw.1, bf16[512,1024]{1,0:T(8,128)(2,1)} %vw.1, f32[64,128]{1,0:T(8,128)} %bitcast.9, f32[1032,128]{1,0:T(8,128)} %constant.4.clone.cos_tab, f32[1032,128]{1,0:T(8,128)} %constant.5.clone.sin_tab, ...), custom_call_target="tpu_custom_call" | custom-call | tf_op jit(solution)/shard_map/pallas_call | solution.py:457
  128.3 2.3 %copy.15 = f32[256,16,64]{0,2,1:T(8,128)} copy(f32[256,16,64]{0,2,1:T(8,128)} %bitcast.8) | data formatting | bytes 2097152
  130.6 1.3 copy.16
